TPU v7x, 256 devices: a whole 4x4x8 slice. The times are simulated.
256 devices in a mesh: ep: 64 (over z, x, core), tp: 4 (over y).
Axes of the slice: x: 4, y: 4, z: 8, core: 2. Of those that a mesh axis runs over, the one named last changes fastest.
Arguments:
- mixer_input: bfloat16 [40960, 2048], P('ep'), may hold values from -6 to 6
- mixer_gain: float32 [2048], replicated, may hold values from 0.1 to 1.9
- value_weight: bfloat16 [2048, 1024], P(None, 'tp'), may hold values from -0.125 to 0.125
- inner_gate: bfloat16 [2048, 1024], P(None, 'tp'), may hold values from -0.125 to 0.125
- outer_gate: bfloat16 [2048, 1024], P(None, 'tp'), may hold values from -0.125 to 0.125
- kernel_taps: float32 [3, 1024], P(None, 'tp'), may hold values from -3 to 3
- mixer_proj: bfloat16 [1024, 2048], P('tp'), may hold values from -0.1875 to 0.1875
- expert_input: bfloat16 [40960, 2048], P(('ep', 'tp')), may hold values from -6 to 6
- expert_gain: float32 [2048], replicated, may hold values from 0.1 to 1.9
- routes: int32 [40960, 2], P(('ep', 'tp')), may hold values from 0 to 63, as said below
- group_logits: float32 [40960, 8], P(('ep', 'tp')), may hold values from -6 to 6
- pair_logits: float32 [40960, 2], P(('ep', 'tp')), may hold values from -6 to 6
- gate_weight: bfloat16 [64, 2048, 1024], P('ep', None, 'tp'), may hold values from -0.125 to 0.125
- up_weight: bfloat16 [64, 2048, 1024], P('ep', None, 'tp'), may hold values from -0.125 to 0.125
- down_weight: bfloat16 [64, 1024, 2048], P('ep', 'tp'), may hold values from -0.75 to 0.75
Outputs:
- mixer_output: bfloat16 [40960, 2048], P(('ep', 'tp'))
- expert_output: bfloat16 [40960, 2048], P(('ep', 'tp'))
Inputs may be any that keep to these rules, and one draw needn't show every extreme that they name: `routes`: both entries of a row are different experts of one group (equal after integer division by 8). In the rows of one device every group is chosen by the same number of rows, no expert is named more than 10 times, and in every draw one expert is named exactly 10 times in the rows of every device.
All inputs are finite; a program needn't handle non-finite values.
Results may differ from a plain program's by a relative error of at most 0.01.
Values may be sent and summed in bfloat16 or wider, within the bound.
A program may use at most 128 MiB of HBM per device.

v0:
```python
import jax
import jax.numpy as jnp
from jax import lax
from jax.sharding import PartitionSpec as P

EPG = 8
EPSILON = 1e-06


def padded_2(cells, axis):
    count = lax.axis_size(axis)
    ends = count - 1
    head = cells[:1]
    tail = cells[-1:]
    return jnp.concatenate(
        [
            lax.ppermute(tail, axis, [(i, i + 1) for i in range(ends)]),
            cells,
            lax.ppermute(head, axis, [(i + 1, i) for i in range(ends)]),
        ],
        axis=0,
    )


def normed(values, gain):
    wide = values.astype(jnp.float32)
    scale = lax.rsqrt(jnp.mean(wide * wide, axis=-1, keepdims=True) + EPSILON)
    return (wide * scale * gain).astype(jnp.bfloat16)


def route_weights(routes, group_logits, pair_logits):
    chosen = routes[:, 0] // EPG
    groups = jnp.arange(group_logits.shape[1], dtype=jnp.int32)
    picked = jnp.sum(jnp.where(groups[None, :] == chosen[:, None], group_logits, 0.0), axis=1)
    group_weight = 1.0 / jnp.sum(jnp.exp(group_logits - picked[:, None]), axis=1)
    return group_weight[:, None] * jax.nn.sigmoid(pair_logits - pair_logits[:, ::-1])


def f32dot(a, b):
    return jnp.dot(a, b, preferred_element_type=jnp.float32)


def on_device(
    mixer_input,
    mixer_gain,
    value_weight,
    inner_gate,
    outer_gate,
    kernel_taps,
    mixer_proj,
    expert_input,
    expert_gain,
    routes,
    group_logits,
    pair_logits,
    gate_weight,
    up_weight,
    down_weight,
):
    split = lax.axis_size("tp")
    experts = lax.axis_size("ep")
    n_groups = experts // EPG
    local = expert_input.shape[0]
    width = expert_input.shape[1]
    per = local // n_groups
    expert_norm = normed(expert_input, expert_gain)
    weights = route_weights(routes, group_logits, pair_logits)
    member = routes % EPG
    lanes = jnp.arange(EPG, dtype=jnp.int32)
    wide_w = jnp.where(member[:, 0:1] == lanes, weights[:, 0:1], 0.0) + jnp.where(
        member[:, 1:2] == lanes, weights[:, 1:2], 0.0
    )
    high = wide_w.astype(jnp.bfloat16)
    low = (wide_w - high.astype(jnp.float32)).astype(jnp.bfloat16)
    extra = jnp.concatenate([high, low, jnp.zeros((local, 128 - 2 * EPG), jnp.bfloat16)], axis=1)
    group = routes[:, 0] // EPG
    place = jnp.arange(local, dtype=jnp.int32)
    earlier = (group[:, None] == group[None, :]) & (place[None, :] < place[:, None])
    slot = group * per + jnp.sum(earlier.astype(jnp.int32), axis=1)
    onehot = (slot[:, None] == place[None, :]).astype(jnp.bfloat16)
    rows = jnp.concatenate([expert_norm, extra], axis=1)
    ordered = lax.dot_general(
        onehot, rows, (((0,), (0,)), ((), ())), preferred_element_type=jnp.float32
    ).astype(jnp.bfloat16)
    z_groups = [[z * EPG + i for z in range(n_groups)] for i in range(EPG)]
    plane_groups = [[z * EPG + i for i in range(EPG)] for z in range(n_groups)]
    arrived = lax.all_to_all(
        ordered, "ep", split_axis=0, concat_axis=0, axis_index_groups=z_groups, tiled=True
    )
    everyone = lax.all_gather(arrived, "ep", axis=0, axis_index_groups=plane_groups, tiled=True)
    all_gate = lax.all_gather(gate_weight[0], "tp", axis=0)
    all_up = lax.all_gather(up_weight[0], "tp", axis=0)
    all_down = lax.all_gather(down_weight[0], "tp", axis=0, tiled=True)
    normal_rows = normed(mixer_input, mixer_gain)
    values = f32dot(normal_rows, value_weight)
    inner = f32dot(normal_rows, inner_gate)
    outer = f32dot(normal_rows, outer_gate)
    mixed_in = (inner * values).astype(jnp.bfloat16)
    padded = padded_2(mixed_in, "ep").astype(jnp.float32)
    conv_sum = (
        kernel_taps[0] * padded[:-2] + kernel_taps[1] * padded[1:-1] + kernel_taps[2] * padded[2:]
    )
    mixer_rows = (outer * conv_sum).astype(jnp.bfloat16)
    partial = f32dot(mixer_rows, mixer_proj).astype(jnp.bfloat16)
    blocks = lax.all_to_all(partial.reshape(split, -1, width), "tp", 0, 0, tiled=True)
    mixer_output = jnp.sum(blocks.astype(jnp.float32), axis=0).astype(jnp.bfloat16)
    tokens = everyone[:, :width]
    mine = lax.axis_index("ep") % EPG
    both = everyone[:, width:].astype(jnp.float32)
    spot = jnp.arange(128, dtype=jnp.int32)
    weight = jnp.sum(
        jnp.where((spot == mine) | (spot == mine + EPG), both, 0.0), axis=1, keepdims=True
    )
    parts = []
    for j in range(split):
        first = f32dot(tokens, all_gate[j])
        second = f32dot(tokens, all_up[j])
        parts.append((jax.nn.silu(first) * second).astype(jnp.bfloat16))
    hidden = jnp.concatenate(parts, axis=1)
    answers = (f32dot(hidden, all_down) * weight).astype(jnp.bfloat16)
    home = lax.psum_scatter(
        answers, "ep", scatter_dimension=0, axis_index_groups=plane_groups, tiled=True
    )
    back = lax.all_to_all(
        home, "ep", split_axis=0, concat_axis=0, axis_index_groups=z_groups, tiled=True
    )
    expert_output = f32dot(onehot, back).astype(jnp.bfloat16)
    return (mixer_output, expert_output)


def solution(mesh):
    in_specs = (
        P("ep", None),
        P(),
        P(None, "tp"),
        P(None, "tp"),
        P(None, "tp"),
        P(None, "tp"),
        P("tp", None),
        P(("ep", "tp"), None),
        P(),
        P(("ep", "tp"), None),
        P(("ep", "tp"), None),
        P(("ep", "tp"), None),
        P("ep", None, "tp"),
        P("ep", None, "tp"),
        P("ep", "tp", None),
    )
    out_specs = (P(("ep", "tp"), None), P(("ep", "tp"), None))
    return jax.shard_map(
        on_device, mesh=mesh, in_specs=in_specs, out_specs=out_specs, check_vma=False
    )
```

profile of v0, /device:TPU:3, one launch (start us, length us, event | category | flops | bytes accessed | tf_op | source)
XLA Modules:
  0.0 350.5 jit_solution(15072283598216035923)
XLA Ops:
  11.8 1.3 fusion.15
  13.4 1.3 fusion.17
  15.6 30.7 %all_to_all.29 = bf16[8,20,2176]{2,1,0:T(8,128)(2,1)S(1)} all-to-all(bf16[8,20,2176]{2,1,0:T(8,128)(2,1)S(1)} %all_to_all.20), channel_id=1, replica_groups={{0,32,64,96,128,160,192,224},{4,36,68,100,132,164,196,228},{8,40,72,104..., dimensions={0} | all-to-all | bytes 1392640 | tf_op jit(solution)/shard_map/all_to_all | solution.py:87
  46.3 1.0 all_to_all.22
  49.5 35.9 %all-gather.6.cloned.1.call-done = bf16[1280,2176]{1,0:T(8,128)(2,1)} async-done(((bf16[160,2176]{1,0:T(8,128)(2,1)}), bf16[1280,2176]{1,0:T(8,128)(2,1)}) %all-gather.6.cloned.1.call-update) | async-done | bytes 5570576 | tf_op jit(solution)/shard_map/all_gather | solution.py:90
  85.4 1.1 select_reduce_fusion
  86.5 51.9 %all-gather.8.cloned.1.call-done = bf16[4,2048,256]{2,1,0:T(8,128)(2,1)} async-done(((bf16[1,2048,256]{2,1,0:T(8,128)(2,1)}), bf16[4,2048,256]{2,1,0:T(8,128)(2,1)}) %all-gather.8.cloned.1.call-update) | async-done | bytes 4194320 | tf_op jit(solution)/shard_map/all_gather | solution.py:91
  138.4 5.5 %fusion.23 = f32[1280,256]{0,1:T(8,128)} fusion(bf16[4,2048,256]{2,1,0:T(8,128)(2,1)} %all-gather.8.cloned.1.call-done, bf16[1280,2176]{1,0:T(8,128)(2,1)} %all-gather.6.cloned.1.call-done), kind=kOutput, calls=%fused_computation.45 | convolution fusion | flops 1342177280 | bytes 7602176 | tf_op jit(solution)/shard_map/dot_general | solution.py:40
  144.6 2.7 fusion.22
  147.3 2.7 fusion.21
  150.0 1.6 fusion.20
  151.6 39.8 %all-gather.10.cloned.1.call-done = bf16[4,2048,256]{2,1,0:T(8,128)(2,1)} async-done(((bf16[1,2048,256]{2,1,0:T(8,128)(2,1)}), bf16[4,2048,256]{2,1,0:T(8,128)(2,1)}) %all-gather.10.cloned.1.call-update) | async-done | bytes 4194320 | tf_op jit(solution)/shard_map/all_gather | solution.py:92
  191.4 5.0 %fusion.11 = bf16[1280,256]{0,1:T(8,128)(2,1)S(1)} fusion(f32[1280,256]{0,1:T(8,128)} %fusion.23, bf16[4,2048,256]{2,1,0:T(8,128)(2,1)} %all-gather.10.cloned.1.call-done, bf16[1280,2176]{1,0:T(8,128)(2,1)} %all-gather.6.cloned.1.call-done), kind=kOutput, calls=%fused_computation.20 | convolution fusion | flops 1344143360 | bytes 8257536 | tf_op jit(solution)/shard_map/dot_general | solution.py:40
  196.4 5.2 %fusion.12 = bf16[1280,256]{0,1:T(8,128)(2,1)} fusion(f32[1280,256]{0,1:T(8,128)S(1)} %copy-done.9, bf16[4,2048,256]{2,1,0:T(8,128)(2,1)S(1)} %copy-done.4, bf16[1280,2176]{1,0:T(8,128)(2,1)} %all-gather.6.cloned.1.call-done), kind=kOutput, calls=%fused_computation.21 | convolution fusion | flops 1344143360 | bytes 8257536 | tf_op jit(solution)/shard_map/dot_general | solution.py:40
  201.7 2.6 fusion.13
  204.3 2.8 fusion.14
  207.1 37.1 %all-gather.12.cloned.1.call-done = bf16[1,1024,2048]{2,1,0:T(8,128)(2,1)} async-done(((bf16[1,256,2048]{2,1,0:T(8,128)(2,1)}), bf16[1,1024,2048]{2,1,0:T(8,128)(2,1)}) %all-gather.12.cloned.1.call-update) | async-done | bytes 4194320 | tf_op jit(solution)/shard_map/all_gather | solution.py:93
  244.2 9.9 %multiply_convert_fusion = bf16[1280,2048]{1,0:T(8,128)(2,1)} fusion(f32[1280]{0:T(1024)S(1)} %select_reduce_fusion, bf16[1,1024,2048]{2,1,0:T(8,128)(2,1)} %all-gather.12.cloned.1.call-done, bf16[1280,256]{0,1:T(8,128)(2,1)} %fusion.14, bf16[1280,256]{0,1:T(8,128)(2,1)} %fusion.13, bf16[1280,256]{0,1:T(8,128)(2,1)} %fusion.12, bf16[1280,256]{0,1:T(8,128)(2,1)S(1)} %fusion.11), kind=kOutput, calls=%fused_computation | convolution fusion | flops 5384437760 | bytes 12063744 | tf_op jit(solution)/shard_map/dot_general | solution.py:40
  254.2 2.3 fusion
  256.5 3.1 fusion.46
  260.6 3.8 %collective-permute-start = (bf16[1,256]{1,0:T(2,128)(2,1)S(1)}, bf16[1,256]{1,0:T(2,128)(2,1)S(1)}, u32[]{:S(2)}, u32[]{:S(2)}) collective-permute-start(bf16[1,256]{1,0:T(2,128)(2,1)S(1)} %get-tuple-element.2), channel_id=1, source_target_pairs={{0,4},{4,8},{8,12},{12,16},{16,20},{20,24},{24,28},{28,32},{32,36}... | collective-permute-start | bytes 1544 | tf_op jit(solution)/shard_map/ppermute | solution.py:17
  264.4 1.9 collective-permute-start.1
  266.3 3.3 collective-permute-done.1
  269.8 6.5 %convolution_convert_fusion.1 = bf16[640,2048]{1,0:T(8,128)(2,1)} fusion(bf16[256,2048]{1,0:T(8,128)(2,1)S(1)} %copy-done, bf16[2048,256]{1,0:T(8,128)(2,1)} %param.19, f32[642,256]{1,0:T(8,128)S(1)} %maximum_convert_fusion, f32[256]{0:T(256)S(1)} %bitcast.59, f32[256]{0:T(256)S(1)} %bitcast.60, f32[256]{0:T(256)S(1)} %bitcast.58, ...), kind=kOutput, calls=%fused_computation.8 | convolution fusion | flops 1349877760 | bytes 9321472 | tf_op jit(solution)/shard_map/dot_general | solution.py:40
  276.3 4.6 %all-to-all-start = ((bf16[4,160,2048]{2,1,0:T(8,128)(2,1)}), bf16[4,160,2048]{2,1,0:T(8,128)(2,1)}, u32[]{:S(2)}, u32[]{:S(2)}) async-start(bf16[4,160,2048]{2,1,0:T(8,128)(2,1)} %bitcast.45), calls=%async_computation | async-start | bytes 5242880 | tf_op jit(solution)/shard_map/all_to_all | solution.py:105
  280.9 13.4 %reduce-scatter.2.cloned.1.call-done = bf16[160,2048]{1,0:T(8,128)(2,1)} async-done(((bf16[1280,2048]{1,0:T(8,128)(2,1)}), bf16[160,2048]{1,0:T(8,128)(2,1)}) %reduce-scatter.2.cloned.1.call-update) | async-done | bytes 655376 | tf_op jit(solution)/shard_map/reduce_scatter | solution.py:121
  294.3 2.0 all_to_all.23
  296.4 15.8 %all-to-all-done = bf16[4,160,2048]{2,1,0:T(8,128)(2,1)} async-done(((bf16[4,160,2048]{2,1,0:T(8,128)(2,1)}), bf16[4,160,2048]{2,1,0:T(8,128)(2,1)}, u32[]{:S(2)}, u32[]{:S(2)}) %all-to-all-start) | async-done | bytes 2621472 | tf_op jit(solution)/shard_map/all_to_all | solution.py:105
  312.2 6.7 %all-to-all-start.2 = ((bf16[8,20,2048]{2,1,0:T(8,128)(2,1)}), bf16[8,20,2048]{2,1,0:T(8,128)(2,1)S(1)}, u32[]{:S(2)}, u32[]{:S(2)}) async-start(bf16[8,20,2048]{2,1,0:T(8,128)(2,1)} %all_to_all.23), calls=%async_computation.3 | async-start | bytes 1572864 | tf_op jit(solution)/shard_map/all_to_all | solution.py:124
  318.9 3.3 reduce_sum.69
  322.1 20.4 %all-to-all-done.2 = bf16[8,20,2048]{2,1,0:T(8,128)(2,1)S(1)} async-done(((bf16[8,20,2048]{2,1,0:T(8,128)(2,1)}), bf16[8,20,2048]{2,1,0:T(8,128)(2,1)S(1)}, u32[]{:S(2)}, u32[]{:S(2)}) %all-to-all-start.2) | async-done | bytes 655392 | tf_op jit(solution)/shard_map/all_to_all | solution.py:124
  342.7 1.2 convolution_convert_fusion.2
  (63 shorter events, 9.7 us)
Async XLA Ops:
  7.2 262.6 %copy-start = (bf16[256,2048]{1,0:T(8,128)(2,1)S(1)}, bf16[256,2048]{1,0:T(8,128)(2,1)}, u32[]{:S(2)}) copy-start(bf16[256,2048]{1,0:T(8,128)(2,1)} %param.21) | copy-start | bytes 3145732
  7.2 78.2 %all-gather.6.cloned.1.call-start = ((), (), s32[]{:S(2)}) async-start(), calls=%async_computation.4 | async-start | bytes 6266880 | tf_op jit(solution)/shard_map/all_gather | solution.py:90
  47.3 91.1 %all-gather.8.cloned.1.call-start = ((), (), s32[]{:S(2)}) async-start(), calls=%async_computation.5 | async-start | bytes 5242880 | tf_op jit(solution)/shard_map/all_gather | solution.py:91
  48.1 143.3 %all-gather.10.cloned.1.call-start = ((), (), s32[]{:S(2)}) async-start(), calls=%async_computation.6 | async-start | bytes 5242880 | tf_op jit(solution)/shard_map/all_gather | solution.py:92
  48.8 195.4 %all-gather.12.cloned.1.call-start = ((), (), s32[]{:S(2)}) async-start(), calls=%async_computation.8 | async-start | bytes 5242880 | tf_op jit(solution)/shard_map/all_gather | solution.py:93
  49.4 244.9 %reduce-scatter.2.cloned.1.call-start = ((), (), s32[]{:S(2)}) async-start(), calls=%async_computation.7 | async-start | bytes 5898240 | tf_op jit(solution)/shard_map/reduce_scatter | solution.py:121
  138.4 5.6 %copy-start.2 = (bf16[1280,2176]{1,0:T(8,128)(2,1)S(1)}, bf16[1280,2176]{1,0:T(8,128)(2,1)}, u32[]{:S(2)}) copy-start(bf16[1280,2176]{1,0:T(8,128)(2,1)} %all-gather.6.cloned.1.call-done) | copy-start | bytes 16711684
  138.4 6.1 %copy-start.5 = (bf16[4,2048,256]{2,1,0:T(8,128)(2,1)S(1)}, bf16[4,2048,256]{2,1,0:T(8,128)(2,1)}, u32[]{:S(2)}) copy-start(bf16[4,2048,256]{2,1,0:T(8,128)(2,1)} %all-gather.8.cloned.1.call-done) | copy-start | bytes 12582916
  191.4 5.0 %copy-start.4 = (bf16[4,2048,256]{2,1,0:T(8,128)(2,1)S(1)}, bf16[4,2048,256]{2,1,0:T(8,128)(2,1)}, u32[]{:S(2)}) copy-start(bf16[4,2048,256]{2,1,0:T(8,128)(2,1)} %all-gather.10.cloned.1.call-done) | copy-start | bytes 12582916
  191.4 5.0 %copy-start.9 = (f32[1280,256]{0,1:T(8,128)S(1)}, f32[1280,256]{0,1:T(8,128)}, u32[]{:S(2)}) copy-start(f32[1280,256]{0,1:T(8,128)} %fusion.22) | copy-start | bytes 3932164
  191.4 10.3 %slice-start = ((s8[5570560]{0:T(1024)(128)(4,1)}), s8[4194304]{0:T(1024)(128)(4,1)S(1)}, s32[]{:S(2)}) async-start(s8[5570560]{0:T(1024)(128)(4,1)} %bitcast.46), calls=%async_computation.9 | async-start | bytes 8388608
  196.4 5.3 %slice-start.1 = ((s8[5570560]{0:T(1024)(128)(4,1)}), s8[1376256]{0:T(1024)(128)(4,1)S(1)}, s32[]{:S(2)}) async-start(s8[5570560]{0:T(1024)(128)(4,1)} %bitcast.46), calls=%async_computation.10 | async-start | bytes 2752512
  196.4 5.3 %copy-start.8 = (f32[1280,256]{0,1:T(8,128)S(1)}, f32[1280,256]{0,1:T(8,128)}, u32[]{:S(2)}) copy-start(f32[1280,256]{0,1:T(8,128)} %fusion.21) | copy-start | bytes 3932164
  254.1 2.4 copy-start.7
  256.5 3.1 copy-start.1
  256.5 3.1 copy-start.6
  259.6 6.7 %copy-start.3 = (f32[3,256]{1,0:T(4,128)S(1)}, f32[3,256]{1,0:T(4,128)}, u32[]{:S(2)}) copy-start(f32[3,256]{1,0:T(4,128)} %param.20) | copy-start | bytes 9220
  260.6 5.8 %collective-permute-start = (bf16[1,256]{1,0:T(2,128)(2,1)S(1)}, bf16[1,256]{1,0:T(2,128)(2,1)S(1)}, u32[]{:S(2)}, u32[]{:S(2)}) collective-permute-start(bf16[1,256]{1,0:T(2,128)(2,1)S(1)} %get-tuple-element.2), channel_id=1, source_target_pairs={{0,4},{4,8},{8,12},{12,16},{16,20},{20,24},{24,28},{28,32},{32,36}... | collective-permute-start | bytes 1544 | tf_op jit(solution)/shard_map/ppermute | solution.py:17
  264.4 5.3 %collective-permute-start.1 = (bf16[1,256]{1,0:T(2,128)(2,1)S(1)}, bf16[1,256]{1,0:T(2,128)(2,1)S(1)}, u32[]{:S(2)}, u32[]{:S(2)}) collective-permute-start(bf16[1,256]{1,0:T(2,128)(2,1)S(1)} %get-tuple-element.3), channel_id=1, source_target_pairs={{4,0},{8,4},{12,8},{16,12},{20,16},{24,20},{28,24},{32,28},{36,32}... | collective-permute-start | bytes 1544 | tf_op jit(solution)/shard_map/ppermute | solution.py:19
  276.3 35.9 %all-to-all-start = ((bf16[4,160,2048]{2,1,0:T(8,128)(2,1)}), bf16[4,160,2048]{2,1,0:T(8,128)(2,1)}, u32[]{:S(2)}, u32[]{:S(2)}) async-start(bf16[4,160,2048]{2,1,0:T(8,128)(2,1)} %bitcast.45), calls=%async_computation | async-start | bytes 5242880 | tf_op jit(solution)/shard_map/all_to_all | solution.py:105
  312.2 30.4 %all-to-all-start.2 = ((bf16[8,20,2048]{2,1,0:T(8,128)(2,1)}), bf16[8,20,2048]{2,1,0:T(8,128)(2,1)S(1)}, u32[]{:S(2)}, u32[]{:S(2)}) async-start(bf16[8,20,2048]{2,1,0:T(8,128)(2,1)} %all_to_all.23), calls=%async_computation.3 | async-start | bytes 1572864 | tf_op jit(solution)/shard_map/all_to_all | solution.py:124
Sparse Core Ops, SparseCore 0:
  47.5 37.8 all-gather.5
  87.2 51.2 all-gather.7
  140.2 51.1 all-gather.9
  193.1 51.1 all-gather.11
  254.3 40.0 reduce-scatter.1
where the time goes:
time: 351 us; the launch traced here: 350 us
  waiting for transfers between devices  220 us (63%)
  matrix products  50.3 us (14%)
  blocking collectives  30.7 us (9%)
  starting transfers between devices  17.3 us (5%)
  between operations  14.1 us (4%)
  other arithmetic  13.2 us (4%)
  local copies, waits for them, and re-layouts  5.27 us (2%)
    all_gather x1, waiting for transfers between devices, on_device(): all_gate = lax.all_gather(gate_weight[0], 'tp', axis=0)  51.9 us
    dot_general x13, matrix products, f32dot(): return jnp.dot(a, b, preferred_element_type=jnp.float32)  49.9 us
    all_gather x1, waiting for transfers between devices, on_device(): all_up = lax.all_gather(up_weight[0], 'tp', axis=0)  39.8 us
    all_gather x1, waiting for transfers between devices, on_device(): all_down = lax.all_gather(down_weight[0], 'tp', axis=0, tiled=True)  37.1 us
    all_gather x1, waiting for transfers between devices, on_device(): lax.all_gather(arrived, 'ep', axis=0, axis_index_groups=plane_groups, til...  35.9 us
    all_to_all x1, blocking collectives, on_device(): lax.all_to_all(ordered, 'ep', split_axis=0, concat_axis=0, axis_index_gro...  30.7 us
    all_to_all x1, waiting for transfers between devices, on_device(): lax.all_to_all(home, 'ep', split_axis=0, concat_axis=0, axis_index_groups...  20.4 us
    all_to_all x1, waiting for transfers between devices, on_device(): lax.all_to_all(partial.reshape(split, -1, width), 'tp', 0, 0, tiled=True)  15.8 us
  transfers between devices with their start and end apart: 9, of which 8 were waited for; matrix products, arithmetic and copies ran while one was open for 13% of the time, Pallas kernels for 0%

commit v1 on v0

--- a/solution.py
+++ b/solution.py
@@ -90,7 +90,21 @@
     everyone = lax.all_gather(arrived, "ep", axis=0, axis_index_groups=plane_groups, tiled=True)
     all_gate = lax.all_gather(gate_weight[0], "tp", axis=0)
     all_up = lax.all_gather(up_weight[0], "tp", axis=0)
-    all_down = lax.all_gather(down_weight[0], "tp", axis=0, tiled=True)
+    ways, here, turn = (lax.axis_size("tp"), lax.axis_index("tp"), down_weight[0].shape[0])
+    lengths = [n * ways if d == 0 else n for d, n in enumerate(down_weight[0].shape)]
+    full = lax.dynamic_update_slice_in_dim(
+        jnp.zeros(lengths, down_weight[0].dtype), down_weight[0], here * turn, axis=0
+    )
+    going_up = going_down = down_weight[0]
+    for far in range(1, ways // 2 + 1):
+        going_up = lax.ppermute(going_up, "tp", [(d, (d + 1) % ways) for d in range(ways)])
+        full = lax.dynamic_update_slice_in_dim(full, going_up, (here - far) % ways * turn, axis=0)
+        if 2 * far < ways:
+            going_down = lax.ppermute(going_down, "tp", [(d, (d - 1) % ways) for d in range(ways)])
+            full = lax.dynamic_update_slice_in_dim(
+                full, going_down, (here + far) % ways * turn, axis=0
+            )
+    all_down = full
     normal_rows = normed(mixer_input, mixer_gain)
     values = f32dot(normal_rows, value_weight)
     inner = f32dot(normal_rows, inner_gate)

time: 351 us -> 311 us (0.89)
  waiting for transfers between devices: 220 us -> 170 us
  local copies, waits for them, and re-layouts: 5.27 us -> 14.5 us
    all_gather x1 -> x0, waiting for transfers between devices: 37.1 us -> none  [on_device(): all_down = lax.all_gather(down_weight[0], 'tp', axis=0, tiled=True)]
    ppermute x0 -> x3, waiting for transfers between devices: none -> 36.9 us  [the longest x2 36.9 us: on_device(): lax.ppermute(going_up, 'tp', [(d, (d + 1) % ways) for d in range(ways)])]
    all_gather x1, waiting for transfers between devices: 35.9 us -> 0.01 us  [on_device(): lax.all_gather(arrived, 'ep', axis=0, axis_index_groups=plane_groups, til...]
    all_gather x1, waiting for transfers between devices: 51.9 us -> 39.3 us  [on_device(): all_gate = lax.all_gather(gate_weight[0], 'tp', axis=0)]
    dynamic_update_slice x0 -> x4, local copies, waits for them, and re-layouts: none -> 6.75 us  [the longest x2 3.35 us: on_device(): lax.dynamic_update_slice_in_dim(full, going_up, (here - far) % ways * tur...]
  transfers between devices with their start and end apart: 9 -> 11, of which waited for: 8 -> 8; matrix products, arithmetic and copies ran while one was open for 13% -> 12% of each run, Pallas kernels for 0% -> 0%
where the time goes in v1:
time: 311 us; the launch traced here: 310 us
  waiting for transfers between devices  170 us (55%)
  matrix products  47 us (15%)
  blocking collectives  30.7 us (10%)
  starting transfers between devices  20.2 us (6%)
  local copies, waits for them, and re-layouts  14.5 us (5%)
  between operations  14.1 us (5%)
  other arithmetic  13.3 us (4%)
    dot_general x13, matrix products, f32dot(): return jnp.dot(a, b, preferred_element_type=jnp.float32)  46.5 us
    all_gather x1, waiting for transfers between devices, on_device(): all_up = lax.all_gather(up_weight[0], 'tp', axis=0)  39.8 us
    all_gather x1, waiting for transfers between devices, on_device(): all_gate = lax.all_gather(gate_weight[0], 'tp', axis=0)  39.3 us
    ppermute x2, waiting for transfers between devices, on_device(): lax.ppermute(going_up, 'tp', [(d, (d + 1) % ways) for d in range(ways)])  36.9 us
    all_to_all x1, blocking collectives, on_device(): lax.all_to_all(ordered, 'ep', split_axis=0, concat_axis=0, axis_index_gro...  30.7 us
    all_to_all x1, waiting for transfers between devices, on_device(): lax.all_to_all(home, 'ep', split_axis=0, concat_axis=0, axis_index_groups...  20.4 us
    all_to_all x1, waiting for transfers between devices, on_device(): lax.all_to_all(partial.reshape(split, -1, width), 'tp', 0, 0, tiled=True)  15.4 us
    reduce_scatter x1, waiting for transfers between devices, on_device(): lax.psum_scatter(answers, 'ep', scatter_dimension=0, axis_index_groups=pl...  13.9 us
  transfers between devices with their start and end apart: 11, of which 8 were waited for; matrix products, arithmetic and copies ran while one was open for 12% of the time, Pallas kernels for 0%

profile of v1, /device:TPU:3, one launch (start us, length us, event | category | flops | bytes accessed | tf_op | source)
XLA Modules:
  0.0 310.2 jit_solution(11117163355137888336)
XLA Ops:
  15.6 30.7 %all_to_all.29 = bf16[8,20,2176]{2,1,0:T(8,128)(2,1)S(1)} all-to-all(bf16[8,20,2176]{2,1,0:T(8,128)(2,1)S(1)} %all_to_all.20), channel_id=1, replica_groups={{0,32,64,96,128,160,192,224},{4,36,68,100,132,164,196,228},{8,40,72,104..., dimensions={0} | all-to-all | bytes 1392640 | tf_op jit(solution)/shard_map/all_to_all | solution.py:87
  48.9 1.4 collective-permute-start.2
  50.2 1.5 collective-permute-start.3
  51.8 21.0 %collective-permute-done.2 = bf16[256,2048]{1,0:T(8,128)(2,1)S(1)} collective-permute-done((bf16[256,2048]{1,0:T(8,128)(2,1)}, bf16[256,2048]{1,0:T(8,128)(2,1)S(1)}, u32[]{:S(2)}, u32[]{:S(2)}) %collective-permute-start.2) | collective-permute-done | bytes 1048608 | tf_op jit(solution)/shard_map/ppermute | solution.py:100
  72.9 2.5 broadcast_in_dim.61
  77.5 2.3 constant_dynamic-update-slice_fusion.1
  79.8 15.8 %collective-permute-done.4 = bf16[256,2048]{1,0:T(8,128)(2,1)} collective-permute-done((bf16[256,2048]{1,0:T(8,128)(2,1)S(1)}, bf16[256,2048]{1,0:T(8,128)(2,1)}, u32[]{:S(2)}, u32[]{:S(2)}) %collective-permute-start.4) | collective-permute-done | bytes 1048608 | tf_op jit(solution)/shard_map/ppermute | solution.py:100
  95.6 2.3 constant_dynamic-update-slice_fusion
  99.1 39.3 %all-gather.6.cloned.1.call-done = bf16[4,2048,256]{2,1,0:T(8,128)(2,1)} async-done(((bf16[1,2048,256]{2,1,0:T(8,128)(2,1)}), bf16[4,2048,256]{2,1,0:T(8,128)(2,1)}) %all-gather.6.cloned.1.call-update) | async-done | bytes 4194320 | tf_op jit(solution)/shard_map/all_gather | solution.py:91
  138.4 5.5 %fusion.22 = f32[1280,256]{0,1:T(8,128)} fusion(bf16[4,2048,256]{2,1,0:T(8,128)(2,1)} %all-gather.6.cloned.1.call-done, bf16[1280,2176]{1,0:T(8,128)(2,1)} %all-gather.4.cloned.1.call-done), kind=kOutput, calls=%fused_computation.44 | convolution fusion | flops 1342177280 | bytes 7602176 | tf_op jit(solution)/shard_map/dot_general | solution.py:40
  144.6 2.7 fusion.21
  147.3 2.7 fusion.20
  150.0 1.6 fusion.19
  151.6 39.8 %all-gather.8.cloned.1.call-done = bf16[4,2048,256]{2,1,0:T(8,128)(2,1)} async-done(((bf16[1,2048,256]{2,1,0:T(8,128)(2,1)}), bf16[4,2048,256]{2,1,0:T(8,128)(2,1)}) %all-gather.8.cloned.1.call-update) | async-done | bytes 4194320 | tf_op jit(solution)/shard_map/all_gather | solution.py:92
  191.4 5.0 %fusion.10 = bf16[1280,256]{0,1:T(8,128)(2,1)S(1)} fusion(f32[1280,256]{0,1:T(8,128)} %fusion.22, bf16[4,2048,256]{2,1,0:T(8,128)(2,1)} %all-gather.8.cloned.1.call-done, bf16[1280,2176]{1,0:T(8,128)(2,1)} %all-gather.4.cloned.1.call-done), kind=kOutput, calls=%fused_computation.19 | convolution fusion | flops 1344143360 | bytes 8257536 | tf_op jit(solution)/shard_map/dot_general | solution.py:40
  196.4 4.4 %fusion.11 = bf16[1280,256]{0,1:T(8,128)(2,1)S(1)} fusion(f32[1280,256]{0,1:T(8,128)S(1)} %copy-done.12, bf16[4,2048,256]{2,1,0:T(8,128)(2,1)S(1)} %copy-done.5, bf16[1280,2176]{1,0:T(8,128)(2,1)} %all-gather.4.cloned.1.call-done), kind=kOutput, calls=%fused_computation.20 | convolution fusion | flops 1344143360 | bytes 8257536 | tf_op jit(solution)/shard_map/dot_general | solution.py:40
  200.9 2.0 fusion.12
  202.9 1.8 fusion.13
  204.7 9.7 %multiply_convert_fusion = bf16[1280,2048]{1,0:T(8,128)(2,1)} fusion(bf16[1024,2048]{1,0:T(8,128)(2,1)} %constant_dynamic-update-slice_fusion, f32[1280]{0:T(1024)S(1)} %select_reduce_fusion, bf16[1280,256]{0,1:T(8,128)(2,1)S(1)} %fusion.13, bf16[1280,256]{0,1:T(8,128)(2,1)S(1)} %fusion.12, bf16[1280,256]{0,1:T(8,128)(2,1)S(1)} %fusion.11, ...), kind=kOutput, calls=%fused_computation | convolution fusion | flops 5384437760 | bytes 12063744 | tf_op jit(solution)/shard_map/dot_general | solution.py:40
  214.4 2.4 fusion
  216.9 2.8 fusion.45
  220.6 3.8 %collective-permute-start = (bf16[1,256]{1,0:T(2,128)(2,1)S(1)}, bf16[1,256]{1,0:T(2,128)(2,1)S(1)}, u32[]{:S(2)}, u32[]{:S(2)}) collective-permute-start(bf16[1,256]{1,0:T(2,128)(2,1)S(1)} %get-tuple-element.2), channel_id=1, source_target_pairs={{0,4},{4,8},{8,12},{12,16},{16,20},{20,24},{24,28},{28,32},{32,36}... | collective-permute-start | bytes 1544 | tf_op jit(solution)/shard_map/ppermute | solution.py:17
  224.4 1.9 collective-permute-start.1
  226.4 3.3 %collective-permute-done.1 = bf16[1,256]{1,0:T(2,128)(2,1)S(1)} collective-permute-done((bf16[1,256]{1,0:T(2,128)(2,1)S(1)}, bf16[1,256]{1,0:T(2,128)(2,1)S(1)}, u32[]{:S(2)}, u32[]{:S(2)}) %collective-permute-start.1) | collective-permute-done | bytes 544 | tf_op jit(solution)/shard_map/ppermute | solution.py:19
  229.8 6.2 %convolution_convert_fusion.1 = bf16[640,2048]{1,0:T(8,128)(2,1)} fusion(bf16[256,2048]{1,0:T(8,128)(2,1)S(1)} %copy-done, bf16[2048,256]{1,0:T(8,128)(2,1)S(1)} %copy-done.9, f32[642,256]{1,0:T(8,128)S(1)} %maximum_convert_fusion, f32[256]{0:T(256)S(1)} %bitcast.61, f32[256]{0:T(256)S(1)} %bitcast.62, f32[256]{0:T(256)S(1)} %bitcast.60, ...), kind=kOutput, calls=%fused_computation.7 | convolution fusion | flops 1349877760 | bytes 9321472 | tf_op jit(solution)/shard_map/dot_general | solution.py:40
  236.1 4.6 %all-to-all-start = ((bf16[4,160,2048]{2,1,0:T(8,128)(2,1)}), bf16[4,160,2048]{2,1,0:T(8,128)(2,1)}, u32[]{:S(2)}, u32[]{:S(2)}) async-start(bf16[4,160,2048]{2,1,0:T(8,128)(2,1)} %bitcast.45), calls=%async_computation | async-start | bytes 5242880 | tf_op jit(solution)/shard_map/all_to_all | solution.py:119
  240.7 13.9 %reduce-scatter.2.cloned.1.call-done = bf16[160,2048]{1,0:T(8,128)(2,1)} async-done(((bf16[1280,2048]{1,0:T(8,128)(2,1)}), bf16[160,2048]{1,0:T(8,128)(2,1)}) %reduce-scatter.2.cloned.1.call-update) | async-done | bytes 655376 | tf_op jit(solution)/shard_map/reduce_scatter | solution.py:135
  254.6 2.0 all_to_all.23
  256.6 15.4 %all-to-all-done = bf16[4,160,2048]{2,1,0:T(8,128)(2,1)} async-done(((bf16[4,160,2048]{2,1,0:T(8,128)(2,1)}), bf16[4,160,2048]{2,1,0:T(8,128)(2,1)}, u32[]{:S(2)}, u32[]{:S(2)}) %all-to-all-start) | async-done | bytes 2621472 | tf_op jit(solution)/shard_map/all_to_all | solution.py:119
  271.9 6.7 %all-to-all-start.2 = ((bf16[8,20,2048]{2,1,0:T(8,128)(2,1)}), bf16[8,20,2048]{2,1,0:T(8,128)(2,1)S(1)}, u32[]{:S(2)}, u32[]{:S(2)}) async-start(bf16[8,20,2048]{2,1,0:T(8,128)(2,1)} %all_to_all.23), calls=%async_computation.3 | async-start | bytes 1572864 | tf_op jit(solution)/shard_map/all_to_all | solution.py:138
  278.7 3.3 %reduce_sum.69 = bf16[160,2048]{1,0:T(8,128)(2,1)} reduce(bf16[4,160,2048]{2,1,0:T(8,128)(2,1)} %all-to-all-done, bf16[]{:T(256)} %constant.80.clone.1), dimensions={0}, to_apply=%region_1.2 | reduce | flops 983040 | bytes 3276802 | tf_op jit(solution)/shard_map/reduce_sum | solution.py:120
  281.9 20.4 %all-to-all-done.2 = bf16[8,20,2048]{2,1,0:T(8,128)(2,1)S(1)} async-done(((bf16[8,20,2048]{2,1,0:T(8,128)(2,1)}), bf16[8,20,2048]{2,1,0:T(8,128)(2,1)S(1)}, u32[]{:S(2)}, u32[]{:S(2)}) %all-to-all-start.2) | async-done | bytes 655392 | tf_op jit(solution)/shard_map/all_to_all | solution.py:138
  (77 shorter events, 17.2 us)
Async XLA Ops:
  7.2 222.7 %copy-start = (bf16[256,2048]{1,0:T(8,128)(2,1)S(1)}, bf16[256,2048]{1,0:T(8,128)(2,1)}, u32[]{:S(2)}) copy-start(bf16[256,2048]{1,0:T(8,128)(2,1)} %param.21) | copy-start | bytes 3145732
  7.2 90.8 %all-gather.4.cloned.1.call-start = ((), (), s32[]{:S(2)}) async-start(), calls=%async_computation.4 | async-start | bytes 6266880 | tf_op jit(solution)/shard_map/all_gather | solution.py:90
  47.3 28.0 %copy-start.2 = (bf16[1,256,2048]{2,1,0:T(8,128)(2,1)S(1)}, bf16[1,256,2048]{2,1,0:T(8,128)(2,1)}, u32[]{:S(2)}) copy-start(bf16[1,256,2048]{2,1,0:T(8,128)(2,1)} %param.29) | copy-start | bytes 3145732
  47.3 91.1 %all-gather.6.cloned.1.call-start = ((), (), s32[]{:S(2)}) async-start(), calls=%async_computation.5 | async-start | bytes 5242880 | tf_op jit(solution)/shard_map/all_gather | solution.py:91
  48.1 143.3 %all-gather.8.cloned.1.call-start = ((), (), s32[]{:S(2)}) async-start(), calls=%async_computation.6 | async-start | bytes 5242880 | tf_op jit(solution)/shard_map/all_gather | solution.py:92
  48.8 205.7 %reduce-scatter.2.cloned.1.call-start = ((), (), s32[]{:S(2)}) async-start(), calls=%async_computation.7 | async-start | bytes 5898240 | tf_op jit(solution)/shard_map/reduce_scatter | solution.py:135
  48.9 23.9 %collective-permute-start.2 = (bf16[256,2048]{1,0:T(8,128)(2,1)}, bf16[256,2048]{1,0:T(8,128)(2,1)S(1)}, u32[]{:S(2)}, u32[]{:S(2)}) collective-permute-start(bf16[256,2048]{1,0:T(8,128)(2,1)} %bitcast.46), channel_id=1, source_target_pairs={{0,1},{1,2},{2,3},{3,0},{4,5},{5,6},{6,7},{7,4},{8,9},{9,10},{10,1... | collective-permute-start | bytes 3145736 | tf_op jit(solution)/shard_map/ppermute | solution.py:100
  50.2 27.2 %collective-permute-start.3 = (bf16[256,2048]{1,0:T(8,128)(2,1)}, bf16[256,2048]{1,0:T(8,128)(2,1)}, u32[]{:S(2)}, u32[]{:S(2)}) collective-permute-start(bf16[256,2048]{1,0:T(8,128)(2,1)} %bitcast.47), channel_id=1, source_target_pairs={{0,3},{1,0},{2,1},{3,2},{4,7},{5,4},{6,5},{7,6},{8,11},{9,8},{10,9... | collective-permute-start | bytes 3145736 | tf_op jit(solution)/shard_map/ppermute | solution.py:103
  72.8 22.8 %collective-permute-start.4 = (bf16[256,2048]{1,0:T(8,128)(2,1)S(1)}, bf16[256,2048]{1,0:T(8,128)(2,1)}, u32[]{:S(2)}, u32[]{:S(2)}) collective-permute-start(bf16[256,2048]{1,0:T(8,128)(2,1)S(1)} %collective-permute-done.2), channel_id=1, source_target_pairs={{0,1},{1,2},{2,3},{3,0},{4,5},{5,6},{6,7},{7,4},{8,9},{9,10},{10,1... | collective-permute-start | bytes 3145736 | tf_op jit(solution)/shard_map/ppermute | solution.py:100
  138.4 5.6 %copy-start.3 = (bf16[1280,2176]{1,0:T(8,128)(2,1)S(1)}, bf16[1280,2176]{1,0:T(8,128)(2,1)}, u32[]{:S(2)}) copy-start(bf16[1280,2176]{1,0:T(8,128)(2,1)} %all-gather.4.cloned.1.call-done) | copy-start | bytes 16711684
  138.4 6.1 %copy-start.6 = (bf16[4,2048,256]{2,1,0:T(8,128)(2,1)S(1)}, bf16[4,2048,256]{2,1,0:T(8,128)(2,1)}, u32[]{:S(2)}) copy-start(bf16[4,2048,256]{2,1,0:T(8,128)(2,1)} %all-gather.6.cloned.1.call-done) | copy-start | bytes 12582916
  191.4 5.0 %copy-start.5 = (bf16[4,2048,256]{2,1,0:T(8,128)(2,1)S(1)}, bf16[4,2048,256]{2,1,0:T(8,128)(2,1)}, u32[]{:S(2)}) copy-start(bf16[4,2048,256]{2,1,0:T(8,128)(2,1)} %all-gather.8.cloned.1.call-done) | copy-start | bytes 12582916
  191.4 5.0 %copy-start.12 = (f32[1280,256]{0,1:T(8,128)S(1)}, f32[1280,256]{0,1:T(8,128)}, u32[]{:S(2)}) copy-start(f32[1280,256]{0,1:T(8,128)} %fusion.21) | copy-start | bytes 3932164
  191.4 9.4 %slice-start = ((s8[5570560]{0:T(1024)(128)(4,1)}), s8[4194304]{0:T(1024)(128)(4,1)S(1)}, s32[]{:S(2)}) async-start(s8[5570560]{0:T(1024)(128)(4,1)} %bitcast.48), calls=%async_computation.8 | async-start | bytes 8388608
  196.4 4.4 %slice-start.1 = ((s8[5570560]{0:T(1024)(128)(4,1)}), s8[1376256]{0:T(1024)(128)(4,1)S(1)}, s32[]{:S(2)}) async-start(s8[5570560]{0:T(1024)(128)(4,1)} %bitcast.48), calls=%async_computation.9 | async-start | bytes 2752512
  196.4 4.4 %copy-start.11 = (f32[1280,256]{0,1:T(8,128)S(1)}, f32[1280,256]{0,1:T(8,128)}, u32[]{:S(2)}) copy-start(f32[1280,256]{0,1:T(8,128)} %fusion.20) | copy-start | bytes 3932164
  214.4 2.4 copy-start.7
  214.4 2.5 copy-start.10
  216.8 2.8 copy-start.1
  216.8 2.8 copy-start.8
  219.7 6.7 %copy-start.4 = (f32[3,256]{1,0:T(4,128)S(1)}, f32[3,256]{1,0:T(4,128)}, u32[]{:S(2)}) copy-start(f32[3,256]{1,0:T(4,128)} %param.20) | copy-start | bytes 9220
  219.7 10.2 %copy-start.9 = (bf16[2048,256]{1,0:T(8,128)(2,1)S(1)}, bf16[2048,256]{1,0:T(8,128)(2,1)}, u32[]{:S(2)}) copy-start(bf16[2048,256]{1,0:T(8,128)(2,1)} %param.19) | copy-start | bytes 3145732
  220.6 5.8 %collective-permute-start = (bf16[1,256]{1,0:T(2,128)(2,1)S(1)}, bf16[1,256]{1,0:T(2,128)(2,1)S(1)}, u32[]{:S(2)}, u32[]{:S(2)}) collective-permute-start(bf16[1,256]{1,0:T(2,128)(2,1)S(1)} %get-tuple-element.2), channel_id=1, source_target_pairs={{0,4},{4,8},{8,12},{12,16},{16,20},{20,24},{24,28},{28,32},{32,36}... | collective-permute-start | bytes 1544 | tf_op jit(solution)/shard_map/ppermute | solution.py:17
  224.4 5.3 %collective-permute-start.1 = (bf16[1,256]{1,0:T(2,128)(2,1)S(1)}, bf16[1,256]{1,0:T(2,128)(2,1)S(1)}, u32[]{:S(2)}, u32[]{:S(2)}) collective-permute-start(bf16[1,256]{1,0:T(2,128)(2,1)S(1)} %get-tuple-element.3), channel_id=1, source_target_pairs={{4,0},{8,4},{12,8},{16,12},{20,16},{24,20},{28,24},{32,28},{36,32}... | collective-permute-start | bytes 1544 | tf_op jit(solution)/shard_map/ppermute | solution.py:19
  236.1 35.9 %all-to-all-start = ((bf16[4,160,2048]{2,1,0:T(8,128)(2,1)}), bf16[4,160,2048]{2,1,0:T(8,128)(2,1)}, u32[]{:S(2)}, u32[]{:S(2)}) async-start(bf16[4,160,2048]{2,1,0:T(8,128)(2,1)} %bitcast.45), calls=%async_computation | async-start | bytes 5242880 | tf_op jit(solution)/shard_map/all_to_all | solution.py:119
  271.9 30.4 %all-to-all-start.2 = ((bf16[8,20,2048]{2,1,0:T(8,128)(2,1)}), bf16[8,20,2048]{2,1,0:T(8,128)(2,1)S(1)}, u32[]{:S(2)}, u32[]{:S(2)}) async-start(bf16[8,20,2048]{2,1,0:T(8,128)(2,1)} %all_to_all.23), calls=%async_computation.3 | async-start | bytes 1572864 | tf_op jit(solution)/shard_map/all_to_all | solution.py:138
Sparse Core Ops, SparseCore 0:
  47.5 37.8 all-gather.3
  87.2 51.2 all-gather.5
  140.2 51.1 all-gather.7
  214.5 40.0 reduce-scatter.1
